TPU v7x, 256 devices: a whole 4x4x8 slice. The times are simulated.
256 devices in a mesh: ep: 64 (over z, y, core), tp: 4 (over x).
Axes of the slice: x: 4, y: 4, z: 8, core: 2. Of those that a mesh axis runs over, the one named last changes fastest.
Arguments:
- conv_value: bfloat16 [24576, 2048], P('ep', 'tp'), may hold values from -36 to 36
- conv_gate: bfloat16 [24576, 2048], P('ep', 'tp'), may hold values from -8 to 8
- conv_taps: bfloat16 [31, 2048], P(None, 'tp'), may hold values from -1 to 1
- conv_gain: float32 [2048], P('tp'), may hold values from 0.1 to 1.9
- conv_proj: bfloat16 [2048, 2048], P('tp'), may hold values from -0.125 to 0.125
- moe_tokens: bfloat16 [24576, 2048], P('ep'), may hold values from -6 to 6
- moe_gain: float32 [2048], replicated, may hold values from 0.1 to 1.9
- routes: int32 [24576, 2], P('ep'), may hold values from 0 to 63, all different within a row; in each aligned block of 384 rows (0 to 383, 384 to 767, ...) at most 18 rows name the same one
- route_weights: float32 [24576, 2], P('ep'), may hold values from 0.3 to 3
- expert_gate: bfloat16 [64, 2048, 1024], P('ep', None, 'tp'), may hold values from -0.125 to 0.125
- expert_up: bfloat16 [64, 2048, 1024], P('ep', None, 'tp'), may hold values from -0.125 to 0.125
- expert_down: bfloat16 [64, 1024, 2048], P('ep', 'tp'), may hold values from -0.1875 to 0.1875
- shared_gate: bfloat16 [2048, 256], replicated, may hold values from -0.125 to 0.125
- shared_up: bfloat16 [2048, 256], replicated, may hold values from -0.125 to 0.125
- shared_down: bfloat16 [256, 2048], P(None, 'tp'), may hold values from -0.375 to 0.375
Outputs:
- conv_result: bfloat16 [24576, 2048], P('ep', 'tp')
- moe_result: bfloat16 [24576, 2048], P('ep', 'tp')
Inputs may be any that keep to these rules, and one draw needn't show every extreme that they name: `routes`: each row names 2 different experts. Among the 384 rows of one index of ep (aligned blocks in order) no expert is named more than 18 times, and in some blocks one expert is named exactly 18 times.
All inputs are finite; a program needn't handle non-finite values.
Results may differ from a plain program's by a relative error of at most 0.01.
Values may be sent and summed in bfloat16 or wider, within the bound.
A program may use at most 64 MiB of HBM per device.

v0:
```python
import jax
import jax.numpy as jnp
from jax import lax
from jax.sharding import PartitionSpec as P

epsilon = 1e-05


def passed_along(value, axis, by):
    devices = lax.axis_size(axis)
    pairs = [(i, i + by) for i in range(devices) if 0 <= i + by < devices]
    return lax.ppermute(value, axis, pairs)


def total_of_pieces(value, axis):
    parts = lax.all_gather(value, axis)
    return parts.sum(axis=0)


def shared_hidden_rows(rows, shared_gate, shared_up):
    return (
        jax.nn.silu(jnp.dot(rows, shared_gate, preferred_element_type=jnp.float32))
        * jnp.dot(rows, shared_up, preferred_element_type=jnp.float32)
    ).astype(jnp.bfloat16)


def local(
    conv_value,
    conv_gate,
    conv_taps,
    conv_gain,
    conv_proj,
    moe_tokens,
    moe_gain,
    routes,
    route_weights,
    expert_gate,
    expert_up,
    expert_down,
    shared_gate,
    shared_up,
    shared_down,
):
    model_width = moe_tokens.shape[1]
    tok_rows = conv_value.shape[0]
    kernel = conv_taps.shape[0]
    gated_rows = (
        conv_value.astype(jnp.float32) * jax.nn.sigmoid(conv_gate.astype(jnp.float32))
    ).astype(jnp.bfloat16)
    previous = passed_along(gated_rows[tok_rows - (kernel - 1) :], "ep", 1)
    padded = jnp.concatenate([previous, gated_rows], axis=0).astype(jnp.float32)
    tap_weights = conv_taps.astype(jnp.float32)
    convolved = jnp.zeros(gated_rows.shape, jnp.float32)
    for offset in range(kernel):
        convolved = convolved + tap_weights[offset][None, :] * padded[offset : offset + tok_rows]
    total_sum, square_sum = (
        total_of_pieces(jnp.sum(convolved, axis=1), "tp"),
        total_of_pieces(jnp.sum(convolved * convolved, axis=1), "tp"),
    )
    average = total_sum / model_width
    variance = square_sum / model_width - average * average
    scaled = (
        (convolved - average[:, None]) * lax.rsqrt(variance + epsilon)[:, None] * conv_gain[None, :]
    )
    activated = jax.nn.silu(scaled).astype(jnp.bfloat16)
    conv_partial = jnp.dot(activated, conv_proj, preferred_element_type=jnp.float32)
    tokens = moe_tokens.astype(jnp.float32)
    token_mean = jnp.mean(tokens, axis=1, keepdims=True)
    centered = tokens - token_mean
    token_var = jnp.mean(centered * centered, axis=1, keepdims=True)
    normalized = (centered * lax.rsqrt(token_var + epsilon) * moe_gain[None, :]).astype(
        jnp.bfloat16
    )
    shared_hidden = shared_hidden_rows(normalized, shared_gate, shared_up)
    shared_part = jnp.dot(shared_hidden, shared_down, preferred_element_type=jnp.float32)
    experts = lax.axis_size("ep")
    top_count = routes.shape[1]
    capacity = 3 * tok_rows * top_count // (2 * experts)
    entries = tok_rows * top_count
    flat_routes = routes.reshape(-1)
    one_hot = (flat_routes[:, None] == jnp.arange(experts, dtype=jnp.int32)[None, :]).astype(
        jnp.int32
    )
    before = jnp.cumsum(one_hot, axis=0) - one_hot
    slot_rank = jnp.sum(before * one_hot, axis=1)
    slot_index = flat_routes * capacity + slot_rank
    source_row = (
        jnp.full((experts * capacity,), -1, jnp.int32)
        .at[slot_index]
        .set(jnp.arange(entries, dtype=jnp.int32))
    )
    filled = source_row >= 0
    token_index = jnp.where(filled, source_row // top_count, 0)
    outgoing = jnp.where(filled[:, None], normalized[token_index], jnp.zeros((), jnp.bfloat16))
    outgoing = outgoing.reshape(experts, capacity, model_width)
    quarter = model_width // lax.axis_size("tp")
    first_column = lax.axis_index("tp") * quarter
    column_block = lax.dynamic_slice_in_dim(outgoing, first_column, quarter, 2)
    arrived = lax.all_to_all(column_block, "ep", split_axis=0, concat_axis=0, tiled=True)
    arrived = lax.all_gather(arrived, "tp", axis=2, tiled=True)
    expert_input = arrived.reshape(experts * capacity, model_width)
    hidden = (
        jax.nn.silu(jnp.dot(expert_input, expert_gate[0], preferred_element_type=jnp.float32))
        * jnp.dot(expert_input, expert_up[0], preferred_element_type=jnp.float32)
    ).astype(jnp.bfloat16)
    expert_partial = jnp.dot(hidden, expert_down[0], preferred_element_type=jnp.float32)
    conv_sum, expert_sum = (
        lax.psum_scatter(
            conv_partial.astype(jnp.bfloat16), "tp", scatter_dimension=1, tiled=True
        ).astype(jnp.float32),
        lax.psum_scatter(
            expert_partial.astype(jnp.bfloat16), "tp", scatter_dimension=1, tiled=True
        ).astype(jnp.float32),
    )
    conv_result = conv_sum.astype(jnp.bfloat16)
    expert_rows = expert_sum.astype(jnp.bfloat16).reshape(experts, capacity, expert_sum.shape[1])
    returned = lax.all_to_all(expert_rows, "ep", split_axis=0, concat_axis=0, tiled=True)
    picked = returned.reshape(experts * capacity, returned.shape[2])[slot_index]
    picked = picked.astype(jnp.float32).reshape(tok_rows, top_count, returned.shape[2])
    moe_result = (shared_part + jnp.sum(route_weights[:, :, None] * picked, axis=1)).astype(
        jnp.bfloat16
    )
    return (conv_result, moe_result)


def solution(mesh):
    placed = (
        P("ep", "tp"),
        P("ep", "tp"),
        P(None, "tp"),
        P("tp"),
        P("tp", None),
        P("ep", None),
        P(),
        P("ep", None),
        P("ep", None),
        P("ep", None, "tp"),
        P("ep", None, "tp"),
        P("ep", "tp", None),
        P(),
        P(),
        P(None, "tp"),
    )
    return jax.shard_map(
        local, mesh=mesh, in_specs=placed, out_specs=(P("ep", "tp"), P("ep", "tp")), check_vma=False
    )
```

profile of v0, /device:TPU:1, one launch (start us, length us, event | category | flops | bytes accessed | tf_op | source)
XLA Modules:
  0.0 311.6 jit_solution(3662823600982574159)
XLA Ops:
  7.2 0.0 all-gather.6.cloned.1.call-start
  7.2 1.0 copy.25
  8.2 0.1 eq.29
  8.3 0.1 eq.25
  8.5 0.7 broadcast_multiply_fusion
  9.2 1.8 reduce-window.6
  11.0 0.3 slice_reduce_fusion
  11.3 0.1 copy.24
  11.4 0.2 mul.517
  11.6 0.1 fusion.60
  11.8 3.4 %scatter_custom_fusion = s32[1152]{0:T(1024)S(1)} fusion(s32[768]{0:T(1024)S(1)} %fusion.68, s32[768]{0:T(1024)S(1)} %iota.11, s32[]{:T(128)} %constant.26.clone.1), kind=kCustom, calls=%fused_computation.127 | custom fusion | bytes 4612 | tf_op jit(solution)/shard_map/scatter | solution.py:90
  15.2 1.8 convert_reduce_fusion
  17.1 0.6 fusion.2
  17.6 1.7 fusion.4
  19.3 12.3 %gather_fusion = bf16[1152,2048]{1,0:T(8,128)(2,1)} fusion(bf16[384,2048]{1,0:T(8,128)(2,1)} %fusion.4, s32[2048]{0:T(1024)S(1)} %pad_clamp_fusion), kind=kCustom, calls=%fused_computation | custom fusion | bytes 9441792 | tf_op jit(solution)/shard_map/gather | solution.py:94
  31.6 7.6 %gather.9 = bf16[64,18,2048]{2,1,0:T(8,128)(2,1)} reshape(bf16[1152,2048]{1,0:T(8,128)(2,1)} %gather_fusion) | data formatting | bytes 9437184 | tf_op jit(solution)/shard_map/gather | solution.py:94
  39.2 0.1 broadcast_in_dim.21
  39.3 1.8 dynamic-slice_select_fusion
  41.2 52.1 %all_to_all.10 = bf16[64,18,512]{2,1,0:T(8,128)(2,1)} all-to-all(bf16[64,18,512]{2,1,0:T(8,128)(2,1)S(1)} %dynamic-slice_select_fusion), channel_id=1, replica_groups=mesh['ep'=64,'tp'=4] {'ep'}, dimensions={0} | all-to-all | bytes 2359296 | tf_op jit(solution)/shard_map/all_to_all | solution.py:99
  93.3 0.0 all-gather.6.cloned.1.call-update
  93.3 0.2 reduce-scatter.5.cloned.1.call-start
  93.5 64.9 %all-gather.6.cloned.1.call-done = bf16[64,18,2048]{2,1,0:T(8,128)(2,1)} async-done(((bf16[64,18,512]{2,1,0:T(8,128)(2,1)}), bf16[64,18,2048]{2,1,0:T(8,128)(2,1)}) %all-gather.6.cloned.1.call-update) | async-done | bytes 4718608 | tf_op jit(solution)/shard_map/all_gather | solution.py:100
  158.5 7.8 %reshape.99 = bf16[1152,2048]{1,0:T(8,128)(2,1)} reshape(bf16[64,18,2048]{2,1,0:T(8,128)(2,1)} %all-gather.6.cloned.1.call-done) | data formatting | bytes 9437184 | tf_op jit(solution)/shard_map/reshape | solution.py:101
  166.2 5.1 %fusion.16 = f32[1152,256]{1,0:T(8,128)} fusion(bf16[1152,2048]{1,0:T(8,128)(2,1)} %reshape.99, bf16[1,2048,256]{2,1,0:T(8,128)(2,1)} %param.24), kind=kOutput, calls=%fused_computation.27 | convolution fusion | flops 1207959552 | bytes 6946816 | tf_op jit(solution)/shard_map/dot_general | solution.py:103
  171.3 10.3 %convolution_convert_fusion = bf16[1152,2048]{1,0:T(8,128)(2,1)} fusion(bf16[1152,2048]{1,0:T(8,128)(2,1)} %reshape.99, f32[1152,256]{1,0:T(8,128)} %fusion.16, bf16[1,256,2048]{2,1,0:T(8,128)(2,1)} %param.26, bf16[1,2048,256]{2,1,0:T(8,128)(2,1)} %param.25), kind=kOutput, calls=%fused_computation.3 | convolution fusion | flops 2420047872 | bytes 12713984 | tf_op jit(solution)/shard_map/dot_general | solution.py:106
  181.6 0.0 reduce-scatter.5.cloned.1.call-update
  181.6 0.0 reduce-scatter.3.cloned.1.call-start
  181.7 0.9 copy-done.2
  182.6 0.1 copy-done.3
  182.7 0.2 multiply_convert_fusion.1
  182.9 3.8 %collective-permute-start = (bf16[30,512]{1,0:T(8,128)(2,1)S(1)}, bf16[30,512]{1,0:T(8,128)(2,1)S(1)}, u32[]{:S(2)}, u32[]{:S(2)}) collective-permute-start(bf16[30,512]{1,0:T(8,128)(2,1)S(1)} %slice.265), channel_id=1, source_target_pairs={{0,4},{4,8},{8,12},{12,16},{16,20},{20,24},{24,28},{28,32},{32,36}... | collective-permute-start | bytes 92168 | tf_op jit(solution)/shard_map/ppermute | solution.py:12
  186.9 0.9 collective-permute-done
  187.8 0.1 maximum_convert_fusion
  187.9 3.8 %fusion.72 = (f32[384]{0:T(512)S(1)}, f32[384]{0:T(512)S(1)}, f32[384,512]{1,0:T(8,128)S(1)}) fusion(f32[414,512]{1,0:T(8,128)S(1)} %maximum_convert_fusion, f32[512]{0:T(512)S(1)} %bitcast.100, f32[512]{0:T(512)S(1)} %bitcast.99, f32[512]{0:T(512)S(1)} %bitcast.98, f32[512]{0:T(512)S(1)} %bitcast.97, f32[512]{0:T(512)S(1)} %bitcast.96, ...), kind=kLoop, calls=%fused_computation.138 | loop fusion | flops 12582144 | bytes 25232384 | tf_op jit(solution)/shard_map/reduce_sum | solution.py:57
  191.8 9.1 %all-gather.2 = f32[4,1,384]{2,1,0:T(1,128)S(1)} all-gather(f32[1,1,384]{2,1,0:T(1,128)S(1)} %reshape.130), channel_id=2, replica_groups=mesh['ep'=64,'tp'=4] {'tp'}, dimensions={0}, use_global_device_ids=true | all-gather | bytes 7680 | tf_op jit(solution)/shard_map/all_gather | solution.py:16
  200.9 9.6 %all-gather.3 = f32[4,1,384]{2,1,0:T(1,128)S(1)} all-gather(f32[1,1,384]{2,1,0:T(1,128)S(1)} %reshape.132), channel_id=3, replica_groups=mesh['ep'=64,'tp'=4] {'tp'}, dimensions={0}, use_global_device_ids=true | all-gather | bytes 7680 | tf_op jit(solution)/shard_map/all_gather | solution.py:16
  210.5 2.3 convolution_convert_fusion.1
  212.9 23.5 %reduce-scatter.5.cloned.1.call-done = bf16[1152,512]{1,0:T(8,128)(2,1)} async-done(((bf16[1152,2048]{1,0:T(8,128)(2,1)}), bf16[1152,512]{1,0:T(8,128)(2,1)}) %reduce-scatter.5.cloned.1.call-update) | async-done | bytes 1179664 | tf_op jit(solution)/shard_map/reduce_scatter | solution.py:111
  236.4 3.0 reshape.100
  239.4 11.1 %all-to-all-start.1 = ((bf16[64,18,512]{2,1,0:T(8,128)(2,1)}), bf16[64,18,512]{2,1,0:T(8,128)(2,1)}, u32[]{:S(2)}, u32[]{:S(2)}) async-start(bf16[64,18,512]{2,1,0:T(8,128)(2,1)} %reshape.100), calls=%async_computation.3 | async-start | bytes 3145728 | tf_op jit(solution)/shard_map/all_to_all | solution.py:117
  250.5 0.1 copy.23
  250.7 3.1 fusion.76
  253.7 35.8 %all-to-all-done.1 = bf16[64,18,512]{2,1,0:T(8,128)(2,1)} async-done(((bf16[64,18,512]{2,1,0:T(8,128)(2,1)}), bf16[64,18,512]{2,1,0:T(8,128)(2,1)}, u32[]{:S(2)}, u32[]{:S(2)}) %all-to-all-start.1) | async-done | bytes 1179680 | tf_op jit(solution)/shard_map/all_to_all | solution.py:117
  289.5 2.3 reshape.101
  291.8 3.3 %gather_fusion.1 = bf16[768,512]{1,0:T(8,128)(2,1)} fusion(bf16[1152,512]{1,0:T(8,128)(2,1)S(1)} %reshape.101, s32[1024]{0:T(1024)S(1)} %pad_clamp_fusion.1), kind=kCustom, calls=%fused_computation.1 | custom fusion | bytes 1575936 | tf_op jit(solution)/shard_map/gather | solution.py:118
  295.1 3.0 reshape.102
  298.1 3.6 %multiply_reduce_fusion = f32[384,512]{1,0:T(8,128)S(1)} fusion(f32[384,2,512]{2,1,0:T(2,128)} %reshape.102, f32[384,2]{1,0:T(8,128)S(1)} %copy.23), kind=kLoop, calls=%fused_computation.15 | loop fusion | flops 589824 | bytes 2362368 | tf_op jit(solution)/shard_map/reduce_sum | solution.py:120
  301.7 3.4 %fusion.6 = bf16[384,512]{1,0:T(8,128)(2,1)} fusion(f32[384,512]{1,0:T(8,128)S(1)} %multiply_reduce_fusion, bf16[256,512]{1,0:T(8,128)(2,1)S(1)} %copy-done.7, bf16[384,2048]{1,0:T(8,128)(2,1)} %fusion.4, bf16[2048,256]{1,0:T(8,128)(2,1)} %param.28, f32[384,256]{1,0:T(8,128)} %fusion.76), kind=kOutput, calls=%fused_computation.17 | convolution fusion | flops 504299520 | bytes 4456448 | tf_op jit(solution)/shard_map/dot_general | solution.py:75
  (36 shorter events, 0.3 us)
Async XLA Ops:
  7.2 203.3 %copy-start = (bf16[512,2048]{1,0:T(8,128)(2,1)S(1)}, bf16[512,2048]{1,0:T(8,128)(2,1)}, u32[]{:S(2)}) copy-start(bf16[512,2048]{1,0:T(8,128)(2,1)} %param.19) | copy-start | bytes 6291460
  7.2 151.3 %all-gather.6.cloned.1.call-start = ((), (), s32[]{:S(2)}) async-start(), calls=%async_computation.5 | async-start | bytes 7864320 | tf_op jit(solution)/shard_map/all_gather | solution.py:100
  15.2 1.9 copy-start.1
  15.2 2.4 copy-start.5
  93.3 143.1 %reduce-scatter.5.cloned.1.call-start = ((), (), s32[]{:S(2)}) async-start(), calls=%async_computation.6 | async-start | bytes 5898240 | tf_op jit(solution)/shard_map/reduce_scatter | solution.py:111
  181.6 1.0 copy-start.2
  181.6 1.1 copy-start.3
  181.6 5.2 %copy-start.4 = (bf16[31,512]{1,0:T(8,128)(2,1)S(1)}, bf16[31,512]{1,0:T(8,128)(2,1)}, u32[]{:S(2)}) copy-start(bf16[31,512]{1,0:T(8,128)(2,1)} %param.17) | copy-start | bytes 95236
  181.6 123.5 %reduce-scatter.3.cloned.1.call-start = ((), (), s32[]{:S(2)}) async-start(), calls=%async_computation.4 | async-start | bytes 1966080 | tf_op jit(solution)/shard_map/reduce_scatter | solution.py:108
  182.9 4.9 %collective-permute-start = (bf16[30,512]{1,0:T(8,128)(2,1)S(1)}, bf16[30,512]{1,0:T(8,128)(2,1)S(1)}, u32[]{:S(2)}, u32[]{:S(2)}) collective-permute-start(bf16[30,512]{1,0:T(8,128)(2,1)S(1)} %slice.265), channel_id=1, source_target_pairs={{0,4},{4,8},{8,12},{12,16},{16,20},{20,24},{24,28},{28,32},{32,36}... | collective-permute-start | bytes 92168 | tf_op jit(solution)/shard_map/ppermute | solution.py:12
  187.9 22.6 %copy-start.8 = (f32[512]{0:T(512)S(1)}, f32[512]{0:T(512)}, u32[]{:S(2)}) copy-start(f32[512]{0:T(512)} %param.18) | copy-start | bytes 6148
  239.4 11.1 %copy-start.6 = (f32[384,2]{0,1:T(2,128)S(1)}, f32[384,2]{0,1:T(2,128)}, u32[]{:S(2)}) copy-start(f32[384,2]{0,1:T(2,128)} %param.23) | copy-start | bytes 9220
  239.4 50.1 %all-to-all-start.1 = ((bf16[64,18,512]{2,1,0:T(8,128)(2,1)}), bf16[64,18,512]{2,1,0:T(8,128)(2,1)}, u32[]{:S(2)}, u32[]{:S(2)}) async-start(bf16[64,18,512]{2,1,0:T(8,128)(2,1)} %reshape.100), calls=%async_computation.3 | async-start | bytes 3145728 | tf_op jit(solution)/shard_map/all_to_all | solution.py:117
  298.1 3.6 %copy-start.7 = (bf16[256,512]{1,0:T(8,128)(2,1)S(1)}, bf16[256,512]{1,0:T(8,128)(2,1)}, u32[]{:S(2)}) copy-start(bf16[256,512]{1,0:T(8,128)(2,1)} %param.29) | copy-start | bytes 786436
Sparse Core Ops, SparseCore 0:
  93.4 65.0 all-gather.5
  181.7 54.6 reduce-scatter.4
  239.5 27.0 reduce-scatter.2
where the time goes:
time: 313 us; the launch traced here: 312 us
  waiting for transfers between devices  125 us (40%)
  blocking collectives  70.7 us (23%)
  local copies, waits for them, and re-layouts  45.9 us (15%)
  matrix products  24.2 us (8%)
  other arithmetic  16.4 us (5%)
  starting transfers between devices  15.2 us (5%)
  between operations  14 us (4%)
    all_gather x1, waiting for transfers between devices, local(): arrived = lax.all_gather(arrived, 'tp', axis=2, tiled=True)  64.9 us
    all_to_all x1, blocking collectives, local(): lax.all_to_all(column_block, 'ep', split_axis=0, concat_axis=0, tiled=True)  52.1 us
    all_to_all x1, waiting for transfers between devices, local(): lax.all_to_all(expert_rows, 'ep', split_axis=0, concat_axis=0, tiled=True)  35.8 us
    reduce_scatter x1, waiting for transfers between devices, local(): lax.psum_scatter(expert_partial.astype(jnp.bfloat16), 'tp', scatter_dimen...  23.5 us
    gather x2, local copies, waits for them, and re-layouts, local(): normalized[token_index]  19.9 us
    all_gather x2, blocking collectives, total_of_pieces(): parts = lax.all_gather(value, axis)  18.6 us
    all_to_all x1, starting transfers between devices, local(): lax.all_to_all(expert_rows, 'ep', split_axis=0, concat_axis=0, tiled=True)  11.1 us
    dot_general x1, matrix products, local(): jnp.dot(hidden, expert_down[0], preferred_element_type=jnp.float32)  10.3 us
  transfers between devices with their start and end apart: 5, of which 4 were waited for; matrix products, arithmetic and copies ran while one was open for 9% of the time, Pallas kernels for 0%

commit v1 on v0

--- a/solution.py
+++ b/solution.py
@@ -41,6 +41,10 @@
     shared_up,
     shared_down,
 ):
+
+    def links_define(page, group_axis):
+        return jnp.concatenate(lax.all_gather(page, group_axis), axis=2)
+
     model_width = moe_tokens.shape[1]
     tok_rows = conv_value.shape[0]
     kernel = conv_taps.shape[0]
@@ -97,7 +101,7 @@
     first_column = lax.axis_index("tp") * quarter
     column_block = lax.dynamic_slice_in_dim(outgoing, first_column, quarter, 2)
     arrived = lax.all_to_all(column_block, "ep", split_axis=0, concat_axis=0, tiled=True)
-    arrived = lax.all_gather(arrived, "tp", axis=2, tiled=True)
+    arrived = links_define(arrived, "tp")
     expert_input = arrived.reshape(experts * capacity, model_width)
     hidden = (
         jax.nn.silu(jnp.dot(expert_input, expert_gate[0], preferred_element_type=jnp.float32))

time: 313 us -> 300 us (0.958)
  waiting for transfers between devices: 125 us -> 112 us
  local copies, waits for them, and re-layouts: 45.9 us -> 49.7 us
    all_gather x1, waiting for transfers between devices: 64.9 us -> 51.9 us  [links_define(): return jnp.concatenate(lax.all_gather(page, group_axis), axis=2)]
    reshape x1 -> x0, local copies, waits for them, and re-layouts: 7.77 us -> none  [local(): expert_input = arrived.reshape(experts * capacity, model_width)]
    all_gather x0 -> x1, local copies, waits for them, and re-layouts: none -> 5.98 us  [links_define(): return jnp.concatenate(lax.all_gather(page, group_axis), axis=2)]
    unnamed x22 -> x27, local copies, waits for them, and re-layouts: 2.18 us -> 6.34 us
  transfers between devices with their start and end apart: 5 -> 5, of which waited for: 4 -> 4; matrix products, arithmetic and copies ran while one was open for 9% -> 10% of each run, Pallas kernels for 0% -> 0%
where the time goes in v1:
time: 300 us; the launch traced here: 299 us
  waiting for transfers between devices  112 us (37%)
  blocking collectives  70.6 us (24%)
  local copies, waits for them, and re-layouts  49.7 us (17%)
  matrix products  21.5 us (7%)
  other arithmetic  16.4 us (5%)
  starting transfers between devices  15.4 us (5%)
  between operations  14.1 us (5%)
    all_to_all x1, blocking collectives, local(): lax.all_to_all(column_block, 'ep', split_axis=0, concat_axis=0, tiled=True)  52 us
    all_gather x1, waiting for transfers between devices, links_define(): return jnp.concatenate(lax.all_gather(page, group_axis), axis=2)  51.9 us
    all_to_all x1, waiting for transfers between devices, local(): lax.all_to_all(expert_rows, 'ep', split_axis=0, concat_axis=0, tiled=True)  35.8 us
    reduce_scatter x1, waiting for transfers between devices, local(): lax.psum_scatter(expert_partial.astype(jnp.bfloat16), 'tp', scatter_dimen...  23.3 us
    gather x2, local copies, waits for them, and re-layouts, local(): normalized[token_index]  19.9 us
    all_gather x2, blocking collectives, total_of_pieces(): parts = lax.all_gather(value, axis)  18.6 us
    all_to_all x1, starting transfers between devices, local(): lax.all_to_all(expert_rows, 'ep', split_axis=0, concat_axis=0, tiled=True)  11 us
    dot_general x1, matrix products, local(): jnp.dot(hidden, expert_down[0], preferred_element_type=jnp.float32)  10.3 us
  transfers between devices with their start and end apart: 5, of which 4 were waited for; matrix products, arithmetic and copies ran while one was open for 10% of the time, Pallas kernels for 0%

profile of v1, /device:TPU:1, one launch (start us, length us, event | category | flops | bytes accessed | tf_op | source)
XLA Modules:
  0.0 299.4 jit_solution(15770622330579259457)
XLA Ops:
  7.2 1.0 copy.26
  8.2 0.1 eq.29
  8.3 0.1 eq.25
  8.5 0.7 broadcast_multiply_fusion
  9.2 1.8 reduce-window.6
  11.0 0.3 slice_reduce_fusion
  11.3 0.1 copy.25
  11.4 0.2 mul.517
  11.6 0.1 fusion.60
  11.8 3.4 %scatter_custom_fusion = s32[1152]{0:T(1024)S(1)} fusion(s32[768]{0:T(1024)S(1)} %fusion.68, s32[768]{0:T(1024)S(1)} %iota.11, s32[]{:T(128)} %constant.26.clone.1), kind=kCustom, calls=%fused_computation.127 | custom fusion | bytes 4612 | tf_op jit(solution)/shard_map/scatter | solution.py:94
  15.2 1.8 convert_reduce_fusion
  17.1 0.6 fusion.2
  17.6 1.7 fusion.4
  19.3 12.3 %gather_fusion = bf16[1152,2048]{1,0:T(8,128)(2,1)} fusion(bf16[384,2048]{1,0:T(8,128)(2,1)} %fusion.4, s32[2048]{0:T(1024)S(1)} %pad_clamp_fusion), kind=kCustom, calls=%fused_computation | custom fusion | bytes 9441792 | tf_op jit(solution)/shard_map/gather | solution.py:98
  31.6 7.6 %gather.9 = bf16[64,18,2048]{2,1,0:T(8,128)(2,1)} reshape(bf16[1152,2048]{1,0:T(8,128)(2,1)} %gather_fusion) | data formatting | bytes 9437184 | tf_op jit(solution)/shard_map/gather | solution.py:98
  39.2 0.1 broadcast_in_dim.21
  39.3 1.8 dynamic-slice_select_fusion
  41.2 52.0 %all_to_all.10 = bf16[64,18,512]{2,1,0:T(8,128)(2,1)S(1)} all-to-all(bf16[64,18,512]{2,1,0:T(8,128)(2,1)S(1)} %dynamic-slice_select_fusion), channel_id=1, replica_groups=mesh['ep'=64,'tp'=4] {'ep'}, dimensions={0} | all-to-all | bytes 2359296 | tf_op jit(solution)/shard_map/all_to_all | solution.py:103
  93.2 1.4 copy.29
  94.6 0.2 reduce-scatter.5.cloned.1.call-start
  94.8 51.9 %all-gather.7.cloned.1.call-done = bf16[256,18,512]{2,0,1:T(8,128)(2,1)} async-done(((bf16[64,18,512]{2,0,1:T(8,128)(2,1)}), bf16[256,18,512]{2,0,1:T(8,128)(2,1)}) %all-gather.7.cloned.1.call-update) | async-done | bytes 4718608 | tf_op jit(solution)/shard_map/all_gather | solution.py:46
  146.7 6.0 %copy.30 = bf16[4,64,18,512]{3,0,2,1:T(4,128)(2,1)S(1)} copy(bf16[4,64,18,512]{3,1,0,2:T(8,128)(2,1)} %bitcast.75) | data formatting | bytes 9437184 | tf_op jit(solution)/shard_map/all_gather | solution.py:46
  152.7 2.0 copy.32
  154.7 2.2 copy-done.2
  156.9 2.4 fusion.16
  159.3 10.3 %convolution_convert_fusion = bf16[1152,2048]{1,0:T(8,128)(2,1)} fusion(bf16[1152,2048]{1,0:T(8,128)(2,1)} %bitcast.77, f32[1152,256]{1,0:T(8,128)} %fusion.16, bf16[1,256,2048]{2,1,0:T(8,128)(2,1)} %param.26, bf16[1,2048,256]{2,1,0:T(8,128)(2,1)} %param.25), kind=kOutput, calls=%fused_computation.3 | convolution fusion | flops 2420047872 | bytes 12713984 | tf_op jit(solution)/shard_map/dot_general | solution.py:110
  169.6 0.0 reduce-scatter.3.cloned.1.call-start
  169.6 0.9 copy-done.3
  170.5 0.1 copy-done.4
  170.6 0.2 multiply_convert_fusion.1
  170.9 4.1 %collective-permute-start = (bf16[30,512]{1,0:T(8,128)(2,1)S(1)}, bf16[30,512]{1,0:T(8,128)(2,1)S(1)}, u32[]{:S(2)}, u32[]{:S(2)}) collective-permute-start(bf16[30,512]{1,0:T(8,128)(2,1)S(1)} %slice.265), channel_id=1, source_target_pairs={{0,4},{4,8},{8,12},{12,16},{16,20},{20,24},{24,28},{28,32},{32,36}... | collective-permute-start | bytes 92168 | tf_op jit(solution)/shard_map/ppermute | solution.py:12
  175.0 0.7 collective-permute-done
  175.7 0.1 maximum_convert_fusion
  175.9 3.8 %fusion.72 = (f32[384]{0:T(512)S(1)}, f32[384]{0:T(512)S(1)}, f32[384,512]{1,0:T(8,128)S(1)}) fusion(f32[414,512]{1,0:T(8,128)S(1)} %maximum_convert_fusion, f32[512]{0:T(512)S(1)} %bitcast.109, f32[512]{0:T(512)S(1)} %bitcast.108, f32[512]{0:T(512)S(1)} %bitcast.107, f32[512]{0:T(512)S(1)} %bitcast.106, f32[512]{0:T(512)S(1)} %bitcast.105, ...), kind=kLoop, calls=%fused_computation.138 | loop fusion | flops 12582144 | bytes 25232384 | tf_op jit(solution)/shard_map/reduce_sum | solution.py:61
  179.7 9.1 %all-gather.3 = f32[4,1,384]{2,1,0:T(1,128)S(1)} all-gather(f32[1,1,384]{2,1,0:T(1,128)S(1)} %reshape.131), channel_id=2, replica_groups=mesh['ep'=64,'tp'=4] {'tp'}, dimensions={0}, use_global_device_ids=true | all-gather | bytes 7680 | tf_op jit(solution)/shard_map/all_gather | solution.py:16
  188.8 9.6 %all-gather.4 = f32[4,1,384]{2,1,0:T(1,128)S(1)} all-gather(f32[1,1,384]{2,1,0:T(1,128)S(1)} %reshape.133), channel_id=3, replica_groups=mesh['ep'=64,'tp'=4] {'tp'}, dimensions={0}, use_global_device_ids=true | all-gather | bytes 7680 | tf_op jit(solution)/shard_map/all_gather | solution.py:16
  198.5 2.3 convolution_convert_fusion.1
  200.8 23.3 %reduce-scatter.5.cloned.1.call-done = bf16[1152,512]{1,0:T(8,128)(2,1)} async-done(((bf16[1152,2048]{1,0:T(8,128)(2,1)}), bf16[1152,512]{1,0:T(8,128)(2,1)}) %reduce-scatter.5.cloned.1.call-update) | async-done | bytes 1179664 | tf_op jit(solution)/shard_map/reduce_scatter | solution.py:115
  224.1 3.0 %reshape.100 = bf16[64,18,512]{2,1,0:T(8,128)(2,1)} reshape(bf16[1152,512]{1,0:T(8,128)(2,1)} %reduce-scatter.5.cloned.1.call-done) | data formatting | bytes 2359296 | tf_op jit(solution)/shard_map/reshape | solution.py:120
  227.1 11.0 %all-to-all-start.1 = ((bf16[64,18,512]{2,1,0:T(8,128)(2,1)}), bf16[64,18,512]{2,1,0:T(8,128)(2,1)}, u32[]{:S(2)}, u32[]{:S(2)}) async-start(bf16[64,18,512]{2,1,0:T(8,128)(2,1)} %reshape.100), calls=%async_computation.3 | async-start | bytes 3145728 | tf_op jit(solution)/shard_map/all_to_all | solution.py:121
  238.2 0.1 copy.24
  238.4 3.1 %fusion.76 = f32[384,256]{1,0:T(8,128)} fusion(bf16[384,2048]{1,0:T(8,128)(2,1)} %fusion.4, bf16[2048,256]{1,0:T(8,128)(2,1)} %param.27), kind=kOutput, calls=%fused_computation.141 | convolution fusion | flops 402653184 | bytes 3014656 | tf_op jit(solution)/shard_map/dot_general | solution.py:22
  241.4 35.8 %all-to-all-done.1 = bf16[64,18,512]{2,1,0:T(8,128)(2,1)} async-done(((bf16[64,18,512]{2,1,0:T(8,128)(2,1)}), bf16[64,18,512]{2,1,0:T(8,128)(2,1)}, u32[]{:S(2)}, u32[]{:S(2)}) %all-to-all-start.1) | async-done | bytes 1179680 | tf_op jit(solution)/shard_map/all_to_all | solution.py:121
  277.2 2.3 reshape.101
  279.5 3.3 %gather_fusion.1 = bf16[768,512]{1,0:T(8,128)(2,1)} fusion(bf16[1152,512]{1,0:T(8,128)(2,1)S(1)} %reshape.101, s32[1024]{0:T(1024)S(1)} %pad_clamp_fusion.1), kind=kCustom, calls=%fused_computation.1 | custom fusion | bytes 1575936 | tf_op jit(solution)/shard_map/gather | solution.py:122
  282.8 3.0 reshape.102
  285.8 3.6 %multiply_reduce_fusion = f32[384,512]{1,0:T(8,128)S(1)} fusion(f32[384,2,512]{2,1,0:T(2,128)} %reshape.102, f32[384,2]{1,0:T(8,128)S(1)} %copy.24), kind=kLoop, calls=%fused_computation.15 | loop fusion | flops 589824 | bytes 2362368 | tf_op jit(solution)/shard_map/reduce_sum | solution.py:124
  289.4 3.4 %fusion.6 = bf16[384,512]{1,0:T(8,128)(2,1)} fusion(f32[384,512]{1,0:T(8,128)S(1)} %multiply_reduce_fusion, bf16[256,512]{1,0:T(8,128)(2,1)S(1)} %copy-done.9, bf16[384,2048]{1,0:T(8,128)(2,1)} %fusion.4, bf16[2048,256]{1,0:T(8,128)(2,1)} %param.28, f32[384,256]{1,0:T(8,128)} %fusion.76), kind=kOutput, calls=%fused_computation.17 | convolution fusion | flops 504299520 | bytes 4456448 | tf_op jit(solution)/shard_map/dot_general | solution.py:79
  (42 shorter events, 0.4 us)
Async XLA Ops:
  7.2 191.3 %copy-start = (bf16[512,2048]{1,0:T(8,128)(2,1)S(1)}, bf16[512,2048]{1,0:T(8,128)(2,1)}, u32[]{:S(2)}) copy-start(bf16[512,2048]{1,0:T(8,128)(2,1)} %param.19) | copy-start | bytes 6291460
  7.2 139.5 %all-gather.7.cloned.1.call-start = ((), (), s32[]{:S(2)}) async-start(), calls=%async_computation.6 | async-start | bytes 5898240 | tf_op jit(solution)/shard_map/all_gather | solution.py:46
  15.2 1.9 copy-start.1
  15.2 2.4 copy-start.6
  94.6 129.5 %reduce-scatter.5.cloned.1.call-start = ((), (), s32[]{:S(2)}) async-start(), calls=%async_computation.5 | async-start | bytes 5898240 | tf_op jit(solution)/shard_map/reduce_scatter | solution.py:115
  152.7 4.2 %copy-start.8 = (bf16[1,2048,256]{2,1,0:T(8,128)(2,1)S(1)}, bf16[1,2048,256]{2,1,0:T(8,128)(2,1)}, u32[]{:S(2)}) copy-start(bf16[1,2048,256]{2,1,0:T(8,128)(2,1)} %param.24) | copy-start | bytes 3145732
  154.7 2.2 copy-start.2
  169.5 1.0 copy-start.3
  169.5 1.1 copy-start.4
  169.5 5.4 %copy-start.5 = (bf16[31,512]{1,0:T(8,128)(2,1)S(1)}, bf16[31,512]{1,0:T(8,128)(2,1)}, u32[]{:S(2)}) copy-start(bf16[31,512]{1,0:T(8,128)(2,1)} %param.17) | copy-start | bytes 95236
  169.6 123.3 %reduce-scatter.3.cloned.1.call-start = ((), (), s32[]{:S(2)}) async-start(), calls=%async_computation.4 | async-start | bytes 1966080 | tf_op jit(solution)/shard_map/reduce_scatter | solution.py:112
  170.9 4.9 %collective-permute-start = (bf16[30,512]{1,0:T(8,128)(2,1)S(1)}, bf16[30,512]{1,0:T(8,128)(2,1)S(1)}, u32[]{:S(2)}, u32[]{:S(2)}) collective-permute-start(bf16[30,512]{1,0:T(8,128)(2,1)S(1)} %slice.265), channel_id=1, source_target_pairs={{0,4},{4,8},{8,12},{12,16},{16,20},{20,24},{24,28},{28,32},{32,36}... | collective-permute-start | bytes 92168 | tf_op jit(solution)/shard_map/ppermute | solution.py:12
  175.9 22.6 %copy-start.10 = (f32[512]{0:T(512)S(1)}, f32[512]{0:T(512)}, u32[]{:S(2)}) copy-start(f32[512]{0:T(512)} %param.18) | copy-start | bytes 6148
  227.1 11.1 %copy-start.7 = (f32[384,2]{0,1:T(2,128)S(1)}, f32[384,2]{0,1:T(2,128)}, u32[]{:S(2)}) copy-start(f32[384,2]{0,1:T(2,128)} %param.23) | copy-start | bytes 9220
  227.1 50.0 %all-to-all-start.1 = ((bf16[64,18,512]{2,1,0:T(8,128)(2,1)}), bf16[64,18,512]{2,1,0:T(8,128)(2,1)}, u32[]{:S(2)}, u32[]{:S(2)}) async-start(bf16[64,18,512]{2,1,0:T(8,128)(2,1)} %reshape.100), calls=%async_computation.3 | async-start | bytes 3145728 | tf_op jit(solution)/shard_map/all_to_all | solution.py:121
  285.8 3.6 %copy-start.9 = (bf16[256,512]{1,0:T(8,128)(2,1)S(1)}, bf16[256,512]{1,0:T(8,128)(2,1)}, u32[]{:S(2)}) copy-start(bf16[256,512]{1,0:T(8,128)(2,1)} %param.29) | copy-start | bytes 786436
Sparse Core Ops, SparseCore 0:
  94.7 51.9 all-gather.6
  169.7 54.3 reduce-scatter.4
  227.2 26.9 reduce-scatter.2
